TPU v7x, 512 devices: a whole 4x4x16 slice. The times are simulated.
512 devices in a mesh: sp: 16 (over z), fs: 4 (over y), tp: 8 (over x, core).
Axes of the slice: x: 4, y: 4, z: 16, core: 2. Of those that a mesh axis runs over, the one named last changes fastest.
Arguments:
- tokens: bfloat16 [4, 4096, 2048], P('fs', 'sp'), may hold values from -6 to 6
- norm_gain: float32 [2048], replicated, may hold values from 0.1 to 1.9
- w_state_in: bfloat16 [2048, 1024], P(('sp', 'fs'), 'tp'), may hold values from -0.125 to 0.125
- w_value: bfloat16 [2048, 1024], P(('sp', 'fs'), 'tp'), may hold values from -0.125 to 0.125
- w_outer: bfloat16 [2048, 1024], P(('sp', 'fs'), 'tp'), may hold values from -0.125 to 0.125
- w_inner: bfloat16 [2048, 1024], P(('sp', 'fs'), 'tp'), may hold values from -0.125 to 0.125
- w_state_out: bfloat16 [2048, 1024], P(('sp', 'fs'), 'tp'), may hold values from -0.125 to 0.125
- w_conv_out: bfloat16 [2048, 1024], P(('sp', 'fs'), 'tp'), may hold values from -0.125 to 0.125
- log_step: float32 [64], P('tp'), may hold values from -4.6 to -3.2
- decay_real: float32 [64, 64], P('tp'), may hold values from -5 to 0
- frequency: float32 [64, 64], P('tp'), may hold values from 1 to 192
- step_rate: float32 [4, 4096], P('fs', 'sp'), may hold values from 0.4 to 2.5
- input_real: float32 [64, 64, 16], P('tp'), may hold values from -1 to 1
- input_imag: float32 [64, 64, 16], P('tp'), may hold values from -1 to 1
- read_real: float32 [64, 16, 64], P('tp'), may hold values from -0.75 to 0.75
- read_imag: float32 [64, 16, 64], P('tp'), may hold values from -0.75 to 0.75
- skip_gain: float32 [64, 16], P('tp'), may hold values from -4 to 4
- conv_taps: float32 [3, 1024], P(None, 'tp'), may hold values from -3.5 to 3.5
- initial_state: float32 [4, 2, 64, 64], P('fs', None, 'tp'), may hold values from -6 to 6
Outputs:
- mixed: bfloat16 [4, 4096, 2048], P('fs', ('sp', 'tp'))
- final_state: float32 [4, 2, 64, 64], P('fs', None, 'tp', 'sp')
All inputs are finite; a program needn't handle non-finite values.
Results may differ from a plain program's by a relative error of at most 0.018.
Values may be sent and summed in bfloat16 or wider, within the bound.
A program may use at most 64 MiB of HBM per device.

v0:
```python
import jax
import jax.numpy as jnp
from jax import lax
from jax.sharding import PartitionSpec as P

HIGHEST = lax.Precision.HIGHEST


def in_one_piece(arrays, axis, dim, along):
    ends, at = ([], 0)
    for a in arrays[:-1]:
        at += a.shape[along]
        ends.append(at)
    both = jnp.concatenate(arrays, axis=along)
    return tuple(jnp.split(lax.all_gather(both, axis, axis=dim, tiled=True), ends, axis=along))


def laid_out(parts, dim):
    parts = jnp.moveaxis(parts, 0, dim)
    dims = parts.shape
    return parts.reshape(*dims[:dim], dims[dim] * dims[dim + 1], *dims[dim + 2 :])


def gather_together(arrays, axis, dims):
    ravelled = jnp.concatenate([a.reshape(-1) for a in arrays])
    lines, at, done = (lax.all_gather(ravelled, axis), 0, [])
    for a, dim in zip(arrays, dims):
        parts = lines[:, at : at + a.size].reshape(-1, *a.shape)
        done.append(laid_out(parts, dim))
        at += a.size
    return tuple(done)


def shifted(value, axis, steps):
    count = lax.axis_size(axis)
    initial, last = (max(0, -steps), min(count, count - steps))
    return lax.ppermute(value, axis, [(source, source + steps) for source in range(initial, last)])


def in_blocks(x, dim, length):
    before, after = (x.shape[:dim], x.shape[dim + 1 :])
    return jnp.moveaxis(x.reshape(*before, length, -1, *after), dim, 0)


def summed_on_arrival(x, axis, dim):
    length = lax.axis_size(axis)
    parts = lax.all_to_all(in_blocks(x, dim, length), axis, 0, 0, tiled=True)
    return jnp.sum(parts.astype(jnp.float32), axis=0)


def complex_product(left_real, left_imag, right_real, right_imag):
    return (
        left_real * right_real - left_imag * right_imag,
        left_real * right_imag + left_imag * right_real,
    )


def chain_pair(earlier, later):
    first_real, first_imag = complex_product(later[0], later[1], earlier[0], earlier[1])
    carry_real, carry_imag = complex_product(later[0], later[1], earlier[2], earlier[3])
    return (first_real, first_imag, carry_real + later[2], carry_imag + later[3])


def apply_map(summary, start_real, start_imag):
    moved_real, moved_imag = complex_product(summary[0], summary[1], start_real, start_imag)
    return (moved_real + summary[2], moved_imag + summary[3])


def body(
    tokens,
    norm_gain,
    w_state_in,
    w_value,
    w_outer,
    w_inner,
    w_state_out,
    w_conv_out,
    log_step,
    decay_real,
    frequency,
    step_rate,
    input_real,
    input_imag,
    read_real,
    read_imag,
    skip_gain,
    conv_taps,
    initial_state,
):
    rows = tokens.shape[1]
    features = tokens[0].astype(jnp.float32)
    mean_square = jnp.mean(features * features, axis=-1, keepdims=True)
    normed = (features * lax.rsqrt(mean_square + 1e-06) * norm_gain).astype(jnp.bfloat16)
    weights = in_one_piece(
        (w_state_in, w_value, w_outer, w_inner, w_state_out, w_conv_out), ("sp", "fs"), 0, 1
    )

    def project(matrix):
        return jnp.dot(normed, matrix, preferred_element_type=jnp.float32).astype(jnp.bfloat16)

    state_in = project(weights[0])
    value = project(weights[1])
    outer = project(weights[2])
    inner = project(weights[3])
    groups, states = decay_real.shape
    group = skip_gain.shape[1]
    flat = groups * states
    decay = decay_real.reshape(flat)
    turn_rate = frequency.reshape(flat)
    step = jnp.exp(log_step)[None, :] * step_rate[0][:, None]
    step_flat = jnp.repeat(step, states, axis=1)
    grow = jnp.exp(step_flat * decay)
    angle = step_flat * turn_rate
    bar_real = grow * jnp.cos(angle)
    bar_imag = grow * jnp.sin(angle)
    modulus = decay * decay + turn_rate * turn_rate
    less_real = bar_real - 1.0
    hold_real = (less_real * decay + bar_imag * turn_rate) / modulus
    hold_imag = (bar_imag * decay - less_real * turn_rate) / modulus
    channels = state_in.astype(jnp.float32).reshape(rows, groups, group)
    coupling = jnp.concatenate([input_real, input_imag], axis=1)
    driven = jnp.einsum("tgh,gqh->tgq", channels, coupling, precision=HIGHEST)
    drive_real = driven[:, :, :states].reshape(rows, flat)
    drive_imag = driven[:, :, states:].reshape(rows, flat)
    push_real, push_imag = complex_product(hold_real, hold_imag, drive_real, drive_imag)
    span = 16
    blocks = rows // span
    lower = (
        lax.broadcasted_iota(jnp.int32, (span, span), 0)
        >= lax.broadcasted_iota(jnp.int32, (span, span), 1)
    ).astype(jnp.float32)
    elapsed = jnp.einsum(
        "ts,bsf->btf", lower, step_flat.reshape(blocks, span, flat), precision=HIGHEST
    )
    rise = jnp.exp(decay * elapsed)
    phase = turn_rate * elapsed
    carry_real = rise * jnp.cos(phase)
    carry_imag = rise * jnp.sin(phase)
    fall = jnp.exp(-decay * elapsed)
    undo_real, undo_imag = complex_product(
        fall * jnp.cos(phase),
        -fall * jnp.sin(phase),
        push_real.reshape(blocks, span, flat),
        push_imag.reshape(blocks, span, flat),
    )
    summed = jnp.einsum(
        "ts,cbsf->cbtf", lower, jnp.stack([undo_real, undo_imag]), precision=HIGHEST
    )
    local_real, local_imag = complex_product(carry_real, carry_imag, summed[0], summed[1])
    ends = (carry_real[:, -1], carry_imag[:, -1], local_real[:, -1], local_imag[:, -1])
    inclusive = lax.associative_scan(chain_pair, ends, axis=0)
    unit_row = jnp.ones((1, flat), jnp.float32)
    empty_row = jnp.zeros((1, flat), jnp.float32)
    before = (
        jnp.concatenate([unit_row, inclusive[0][:-1]], axis=0),
        jnp.concatenate([empty_row, inclusive[1][:-1]], axis=0),
        jnp.concatenate([empty_row, inclusive[2][:-1]], axis=0),
        jnp.concatenate([empty_row, inclusive[3][:-1]], axis=0),
    )
    summary = (inclusive[0][-1], inclusive[1][-1], inclusive[2][-1], inclusive[3][-1])
    opening_state = initial_state[0].reshape(2, flat)
    every = gather_together(
        (summary[0][None], summary[1][None], summary[2][None], summary[3][None]), "sp", (0, 0, 0, 0)
    )
    running = lax.associative_scan(chain_pair, every, axis=0)
    position = lax.axis_index("sp")
    earlier = jnp.maximum(position - 1, 0)
    picked = [lax.dynamic_index_in_dim(piece, earlier, 0, keepdims=False) for piece in running]
    opening = position == 0
    prefix = (
        jnp.where(opening, 1.0, picked[0]),
        jnp.where(opening, 0.0, picked[1]),
        jnp.where(opening, 0.0, picked[2]),
        jnp.where(opening, 0.0, picked[3]),
    )
    enter_real, enter_imag = apply_map(prefix, opening_state[0], opening_state[1])
    total_map = (running[0][-1], running[1][-1], running[2][-1], running[3][-1])
    closing_real, closing_imag = apply_map(total_map, opening_state[0], opening_state[1])
    closing = jnp.stack([closing_real, closing_imag])
    block_real, block_imag = apply_map(before, enter_real[None], enter_imag[None])
    shift_real, shift_imag = complex_product(
        carry_real, carry_imag, block_real[:, None], block_imag[:, None]
    )
    hidden_real = (local_real + shift_real).reshape(rows, groups, states)
    hidden_imag = (local_imag + shift_imag).reshape(rows, groups, states)
    reading = jnp.concatenate([read_real, -read_imag], axis=2)
    joined = jnp.concatenate([hidden_real, hidden_imag], axis=2)
    response = jnp.einsum("tgq,ghq->tgh", joined, reading, precision=HIGHEST) + skip_gain * channels
    state_mix = jax.nn.gelu(response).reshape(rows, groups * group).astype(jnp.bfloat16)
    gated = (inner.astype(jnp.float32) * value.astype(jnp.float32)).astype(jnp.bfloat16)
    reach = conv_taps.shape[0] - 1
    earlier_rows = shifted(gated[rows - reach :], "sp", 1)
    extended = jnp.concatenate([earlier_rows, gated], axis=0).astype(jnp.float32)
    filtered = conv_taps[0] * extended[0:rows]
    for tap in range(1, reach + 1):
        filtered = filtered + conv_taps[tap] * extended[tap : tap + rows]
    conv_mix = (outer.astype(jnp.float32) * filtered).astype(jnp.bfloat16)
    mixed = summed_on_arrival(
        (
            jnp.einsum("rc,dc->rd", state_mix, weights[4], preferred_element_type=jnp.float32)
            + jnp.einsum("rc,dc->rd", conv_mix, weights[5], preferred_element_type=jnp.float32)
        ).astype(jnp.bfloat16),
        "tp",
        0,
    ).astype(jnp.bfloat16)
    share = states // lax.axis_size("sp")
    closing_grid = closing.reshape(2, groups, states)
    own_share = lax.dynamic_slice_in_dim(closing_grid, lax.axis_index("sp") * share, share, 2)
    return (mixed[None], own_share[None])


def solution(mesh):
    return jax.shard_map(
        body,
        mesh=mesh,
        in_specs=(
            P("fs", "sp", None),
            P(),
            P(("sp", "fs"), "tp"),
            P(("sp", "fs"), "tp"),
            P(("sp", "fs"), "tp"),
            P(("sp", "fs"), "tp"),
            P(("sp", "fs"), "tp"),
            P(("sp", "fs"), "tp"),
            P("tp"),
            P("tp", None),
            P("tp", None),
            P("fs", "sp"),
            P("tp", None, None),
            P("tp", None, None),
            P("tp", None, None),
            P("tp", None, None),
            P("tp", None),
            P(None, "tp"),
            P("fs", None, "tp", None),
        ),
        out_specs=(P("fs", ("sp", "tp"), None), P("fs", None, "tp", "sp")),
        check_vma=False,
    )
```

profile of v0, /device:TPU:1, one launch (start us, length us, event | category | flops | bytes accessed | tf_op | source)
XLA Modules:
  0.0 255.2 jit_solution(16286001688518768119)
XLA Ops:
  7.2 0.0 copy-start
  7.2 0.0 all-gather.3.cloned.1.call-start
  7.3 0.8 constant_dynamic-update-slice_fusion.5
  8.0 0.7 constant_dynamic-update-slice_fusion.4
  8.8 0.7 constant_dynamic-update-slice_fusion.3
  9.5 0.7 constant_dynamic-update-slice_fusion.2
  10.2 0.7 constant_dynamic-update-slice_fusion.1
  10.9 0.7 constant_dynamic-update-slice_fusion
  11.6 0.6 copy-done.5
  12.2 0.0 all-gather.3.cloned.1.call-update
  12.2 0.7 exp.20
  12.9 0.8 broadcast_multiply_fusion.1
  13.7 0.3 broadcast_in_dim.15
  14.0 0.3 reshape_reshape.3
  14.3 0.1 mul.689
  14.4 0.1 mul.696
  14.5 0.1 squeeze.42
  14.5 0.1 squeeze.43
  14.6 0.0 copy-start.10
  14.7 0.3 fusion.1
  15.0 0.4 fusion.59
  15.4 0.0 copy-start.6
  15.4 2.9 %sine_bitcast_fusion = (f32[16,16,512]{2,0,1:T(8,128)S(1)}, f32[16,512,16]{1,0,2:T(8,128)}, f32[16,16,512]{2,0,1:T(8,128)S(1)}) fusion(f32[16,512,16]{1,2,0:T(8,128)S(1)} %fusion.59, f32[512]{0:T(512)S(1)} %mul.696, f32[512]{0:T(512)S(1)} %mul.689), kind=kLoop, calls=%fused_computation.50 | loop fusion | flops 262144 | bytes 2101248 | tf_op jit(solution)/shard_map/sin | solution.py:142
  18.3 133.8 %all-gather.3.cloned.1.call-done = bf16[2048,768]{1,0:T(8,128)(2,1)} async-done(((bf16[32,768]{1,0:T(8,128)(2,1)}), bf16[2048,768]{1,0:T(8,128)(2,1)}) %all-gather.3.cloned.1.call-update) | async-done | bytes 3145744 | tf_op jit(solution)/shard_map/all_gather | solution.py:15
  152.1 1.9 convolution_convert_fusion.3
  154.1 0.7 convolution_bitcast_fusion
  154.8 0.1 fusion.82
  154.9 1.3 copy.62
  156.3 1.5 reshape.174
  157.8 1.3 copy.63
  159.1 2.3 reshape.175
  161.4 4.1 %subtract_bitcast_fusion = (f32[1,16,16,512]{3,2,1,0:T(8,128)S(1)}, f32[1,16,16,512]{3,2,1,0:T(8,128)S(1)}, f32[16,16,512]{2,1,0:T(8,128)S(1)}) fusion(f32[16,512,16]{1,0,2:T(8,128)} %get-tuple-element.14, f32[16,512,16]{1,2,0:T(8,128)S(1)} %fusion.59, f32[512]{0:T(512)S(1)} %get-tuple-element.118, f32[16,16,512]{2,0,1:T(8,128)S(1)} %get-tuple-element.13, ...), kind=kLoop, calls=%fused_computation.48 | loop fusion | flops 3932160 | bytes 5251072 | tf_op jit(solution)/shard_map/stack | solution.py:147
  165.5 0.6 fusion.12
  166.2 0.6 copy.110
  166.8 1.4 multiply_subtract_fusion
  168.1 0.1 fusion.29
  168.2 0.6 copy_add_fusion.1
  169.0 0.8 slice_bitcast_fusion.4
  171.4 21.3 %all-gather = f32[32768]{0:T(1024)S(1)} all-gather(f32[2048]{0:T(1024)S(1)} %pad_maximum_fusion.12), channel_id=2, replica_groups=mesh['sp'=16,'fs'=4,'tp'=8] {'sp'}, dimensions={0}, use_global_device_ids=true | all-gather | bytes 139264 | tf_op jit(solution)/shard_map/all_gather | solution.py:26
  194.7 0.1 add_reduce_fusion.1
  194.8 1.2 subtract_add_fusion
  196.0 0.3 copy.72
  196.3 0.2 reshape.176
  196.6 0.2 copy.75
  196.8 0.6 copy-done.3
  197.4 0.3 copy-done.4
  197.6 1.2 fusion.28
  198.8 1.3 reshape.177
  200.2 0.2 copy.76
  200.4 0.0 copy-start.8
  200.4 0.0 copy-start.12
  200.4 1.6 fusion.8
  202.0 1.5 fusion.7
  203.6 1.9 collective-permute-start
  205.5 1.2 fusion.41
  206.7 1.5 fusion.24
  208.2 3.0 %fusion = bf16[256,2048]{1,0:T(8,128)(2,1)} fusion(f32[256,2048]{1,0:T(8,128)S(1)} %fusion.24, bf16[2048,768]{1,0:T(8,128)(2,1)} %all-gather.3.cloned.1.call-done, f32[258,128]{1,0:T(8,128)S(1)} %maximum_convert_fusion, f32[128]{0:T(128)S(1)} %get-tuple-element.115, f32[128]{0:T(128)S(1)} %get-tuple-element.116, f32[128]{0:T(128)S(1)} %get-tuple-element.114, ...), kind=kOutput, calls=%fused_computation.3 | convolution fusion | flops 271876096 | bytes 5646848 | tf_op jit(solution)/shard_map/rc,dc->rd/dot_general | solution.py:201
  211.3 21.2 %all-to-all-start = ((bf16[8,32,2048]{2,1,0:T(8,128)(2,1)}), bf16[8,32,2048]{2,1,0:T(8,128)(2,1)S(1)}, u32[]{:S(2)}, u32[]{:S(2)}) async-start(bf16[8,32,2048]{2,1,0:T(8,128)(2,1)} %bitcast.114), calls=%async_computation | async-start | bytes 2097152 | tf_op jit(solution)/shard_map/all_to_all | solution.py:47
  232.5 0.1 stack.21
  232.6 0.1 stack.22
  232.7 0.1 dynamic-slice_maximum_fusion
  232.8 0.7 copy.77
  233.4 14.1 %all-to-all-done = bf16[8,32,2048]{2,1,0:T(8,128)(2,1)S(1)} async-done(((bf16[8,32,2048]{2,1,0:T(8,128)(2,1)}), bf16[8,32,2048]{2,1,0:T(8,128)(2,1)S(1)}, u32[]{:S(2)}, u32[]{:S(2)}) %all-to-all-start) | async-done | bytes 1048608 | tf_op jit(solution)/shard_map/all_to_all | solution.py:47
  247.5 0.8 reduce_sum.22
  (253 shorter events, 3.0 us)
Async XLA Ops:
  7.2 7.1 %copy-start.13 = (f32[8,64]{1,0:T(8,128)S(1)}, f32[8,64]{1,0:T(8,128)}, u32[]{:S(2)}) copy-start(f32[8,64]{1,0:T(8,128)} %param.28) | copy-start | bytes 6148
  7.2 7.2 %copy-start.14 = (f32[8,64]{1,0:T(8,128)S(1)}, f32[8,64]{1,0:T(8,128)}, u32[]{:S(2)}) copy-start(f32[8,64]{1,0:T(8,128)} %param.29) | copy-start | bytes 6148
  7.2 7.3 %copy-start.11 = (f32[1,2,8,64]{3,2,1,0:T(8,128)S(1)}, f32[1,2,8,64]{3,2,1,0:T(8,128)}, u32[]{:S(2)}) copy-start(f32[1,2,8,64]{3,2,1,0:T(8,128)} %param.37) | copy-start | bytes 12292
  7.2 7.4 %copy-start.9 = (f32[8,16,64]{2,1,0:T(8,128)S(1)}, f32[8,16,64]{2,1,0:T(8,128)}, u32[]{:S(2)}) copy-start(f32[8,16,64]{2,1,0:T(8,128)} %param.34) | copy-start | bytes 98308
  7.2 7.4 %copy-start = (bf16[1,256,2048]{2,1,0:T(8,128)(2,1)S(1)}, bf16[1,256,2048]{2,1,0:T(8,128)(2,1)}, u32[]{:S(2)}) copy-start(bf16[1,256,2048]{2,1,0:T(8,128)(2,1)} %param.19) | copy-start | bytes 3145732
  7.2 144.9 %all-gather.3.cloned.1.call-start = ((), (), s32[]{:S(2)}) async-start(), calls=%async_computation.1 | async-start | bytes 3194880 | tf_op jit(solution)/shard_map/all_gather | solution.py:15
  10.9 4.1 %copy-start.15 = (f32[3,128]{1,0:T(4,128)S(1)}, f32[3,128]{1,0:T(4,128)}, u32[]{:S(2)}) copy-start(f32[3,128]{1,0:T(4,128)} %param.36) | copy-start | bytes 4612
  11.6 0.6 copy-start.5
  14.6 137.5 %copy-start.10 = (f32[2048]{0:T(1024)S(1)}, f32[2048]{0:T(1024)}, u32[]{:S(2)}) copy-start(f32[2048]{0:T(1024)} %param.20) | copy-start | bytes 24580
  15.4 138.7 %copy-start.6 = (f32[8,64,16]{1,2,0:T(8,128)S(1)}, f32[8,64,16]{1,2,0:T(8,128)}, u32[]{:S(2)}) copy-start(f32[8,64,16]{1,2,0:T(8,128)} %param.32) | copy-start | bytes 98308
  15.4 138.7 %copy-start.7 = (f32[8,64,16]{1,2,0:T(8,128)S(1)}, f32[8,64,16]{1,2,0:T(8,128)}, u32[]{:S(2)}) copy-start(f32[8,64,16]{1,2,0:T(8,128)} %param.31) | copy-start | bytes 98308
  168.8 24.1 %copy-start.2 = (f32[16,16,512]{2,1,0:T(8,128)}, f32[16,16,512]{2,1,0:T(8,128)S(1)}, u32[]{:S(2)}) copy-start(f32[16,16,512]{2,1,0:T(8,128)S(1)} %copy_add_fusion.1) | copy-start | bytes 1572868
  196.3 1.0 copy-start.3
  196.6 1.1 copy-start.4
  198.8 1.6 copy-start.1
  200.4 5.1 %copy-start.8 = (f32[8,16,64]{2,1,0:T(8,128)S(1)}, f32[8,16,64]{2,1,0:T(8,128)}, u32[]{:S(2)}) copy-start(f32[8,16,64]{2,1,0:T(8,128)} %param.33) | copy-start | bytes 98308
  200.4 5.1 %copy-start.12 = (f32[8,16]{1,0:T(8,128)S(1)}, f32[8,16]{1,0:T(8,128)}, u32[]{:S(2)}) copy-start(f32[8,16]{1,0:T(8,128)} %param.35) | copy-start | bytes 1540
  203.6 4.7 %collective-permute-start = (bf16[2,128]{1,0:T(2,128)(2,1)S(1)}, bf16[2,128]{1,0:T(2,128)(2,1)S(1)}, u32[]{:S(2)}, u32[]{:S(2)}) collective-permute-start(bf16[2,128]{1,0:T(2,128)(2,1)S(1)} %slice.852), channel_id=1, source_target_pairs={{0,32},{32,64},{64,96},{96,128},{128,160},{160,192},{192,224},{224... | collective-permute-start | bytes 1544 | tf_op jit(solution)/shard_map/ppermute | solution.py:37
  211.3 36.2 %all-to-all-start = ((bf16[8,32,2048]{2,1,0:T(8,128)(2,1)}), bf16[8,32,2048]{2,1,0:T(8,128)(2,1)S(1)}, u32[]{:S(2)}, u32[]{:S(2)}) async-start(bf16[8,32,2048]{2,1,0:T(8,128)(2,1)} %bitcast.114), calls=%async_computation | async-start | bytes 2097152 | tf_op jit(solution)/shard_map/all_to_all | solution.py:47
Sparse Core Ops, SparseCore 0:
  12.4 139.7 all-gather.2
where the time goes:
time: 256 us; the launch traced here: 255 us
  waiting for transfers between devices  148 us (58%)
  starting transfers between devices  23.2 us (9%)
  blocking collectives  21.3 us (8%)
  local copies, waits for them, and re-layouts  20.6 us (8%)
  between operations  15.4 us (6%)
  other arithmetic  14.3 us (6%)
  matrix products  12.5 us (5%)
    all_gather x1, waiting for transfers between devices, in_one_piece(): lax.all_gather(both, axis, axis=dim, tiled=True)  134 us
    all_gather x1, blocking collectives, gather_together(): lines, at, done = (lax.all_gather(ravelled, axis), 0, [])  21.3 us
    all_to_all x1, starting transfers between devices, summed_on_arrival(): parts = lax.all_to_all(in_blocks(x, dim, length), axis, 0, 0, tiled=True)  21.2 us
    all_to_all x1, waiting for transfers between devices, summed_on_arrival(): parts = lax.all_to_all(in_blocks(x, dim, length), axis, 0, 0, tiled=True)  14.1 us
    unnamed x45, local copies, waits for them, and re-layouts  5.2 us
  transfers between devices with their start and end apart: 3, of which 2 were waited for; matrix products, arithmetic and copies ran while one was open for 4% of the time, Pallas kernels for 0%

commit v1 on v0

--- a/solution.py
+++ b/solution.py
@@ -1,9 +1,139 @@
 import jax
 import jax.numpy as jnp
 from jax import lax
+from jax.experimental import pallas as pl
+from jax.experimental.pallas import tpu as pltpu
 from jax.sharding import PartitionSpec as P
 
+
 HIGHEST = lax.Precision.HIGHEST
+MESH = pl.DeviceIdType.MESH
+NZ, NY = 16, 4
+
+
+def gather_kernel(*refs):
+    shards = refs[:6]
+    wg = refs[6]
+    lsem, ya_s, ya_r, az_s, az_r, bz_s, bz_r, by_s, by_r = refs[7:]
+    z = lax.axis_index("sp")
+    y = lax.axis_index("fs")
+    t = lax.axis_index("tp")
+    zn, zp = lax.rem(z + 1, NZ), lax.rem(z + NZ - 1, NZ)
+
+    barrier = pltpu.get_barrier_semaphore()
+    for d in range(1, NY):
+        pl.semaphore_signal(barrier, inc=1, device_id=(z, lax.rem(y + d, NY), t), device_id_type=MESH)
+    for n in (zn, zp):
+        pl.semaphore_signal(barrier, inc=1, device_id=(n, y, t), device_id_type=MESH)
+
+    mine = pl.ds(pl.multiple_of(y * 32, 32), 32)
+    local = [pltpu.make_async_copy(shards[w], wg.at[w, z, mine, :], lsem.at[w]) for w in range(6)]
+    for c in local:
+        c.start()
+    pl.semaphore_wait(barrier, NY - 1 + 2)
+    for c in local:
+        c.wait()
+
+    def a_y(d):
+        return pltpu.make_async_remote_copy(
+            wg.at[pl.ds(0, 3), z, mine, :], wg.at[pl.ds(0, 3), z, mine, :], ya_s.at[d - 1], ya_r.at[d - 1],
+            device_id=(z, lax.rem(y + d, NY), t), device_id_type=MESH)
+
+    def b_y(k, d):
+        zb = lax.rem(z + k + NZ, NZ)
+        return pltpu.make_async_remote_copy(
+            wg.at[pl.ds(3, 3), zb, mine, :], wg.at[pl.ds(3, 3), zb, mine, :], by_s.at[zb, d - 1], by_r.at[zb, d - 1],
+            device_id=(z, lax.rem(y + d, NY), t), device_id_type=MESH)
+
+    def b_z(k, side):
+        zb = lax.rem(z + (k if side else NZ - k), NZ)
+        return pltpu.make_async_remote_copy(
+            wg.at[pl.ds(3, 3), zb, mine, :], wg.at[pl.ds(3, 3), zb, mine, :], bz_s.at[side, k], bz_r.at[side, k],
+            device_id=(zp if side else zn, y, t), device_id_type=MESH)
+
+    def a_z(k, side, w):
+        zb = lax.rem(z + (k if side else NZ - k), NZ)
+        return pltpu.make_async_remote_copy(
+            wg.at[w, zb], wg.at[w, zb], az_s.at[side, w, k], az_r.at[side, w, k],
+            device_id=(zp if side else zn, y, t), device_id_type=MESH)
+
+    for d in (2, 1, 3):
+        a_y(d).start()
+    for side in (0, 1):
+        b_z(0, side).start()
+    for d in (2, 1, 3):
+        b_y(0, d).start()
+    for d in (1, 3, 2):
+        a_y(d).wait_recv()
+    for w in range(3):
+        for side in (0, 1):
+            a_z(0, side, w).start()
+
+    def step(k, right, left):
+        sides = [s for s, on in ((0, right), (1, left)) if on is not None]
+        fwd = {0: right, 1: left}
+        for s in sides:
+            b_z(k - 1, s).wait_recv()
+            if fwd[s]:
+                b_z(k, s).start()
+            for d in (2, 1, 3):
+                b_y(k if s else -k, d).start()
+        for w in range(3):
+            for s in sides:
+                a_z(k - 1, s, w).wait_recv()
+                if fwd[s]:
+                    a_z(k, s, w).start()
+
+    def loop(k, c):
+        step(k, True, True)
+        return c
+
+    lax.fori_loop(1, 7, loop, 0)
+    step(7, True, False)
+    step(8, False, None)
+
+    def drain_y(k, c):
+        for d in (1, 2, 3):
+            b_y(k, d).wait()
+        return c
+
+    lax.fori_loop(0, NZ, drain_y, 0)
+    for d in (1, 2, 3):
+        a_y(d).wait_send()
+
+    def drain(k, c):
+        for s in (0, 1):
+            b_z(k, s).wait_send()
+            for w in range(3):
+                a_z(k, s, w).wait_send()
+        return c
+
+    lax.fori_loop(0, 7, drain, 0)
+    b_z(7, 0).wait_send()
+    for w in range(3):
+        a_z(7, 0, w).wait_send()
+
+
+def gather_weights(shards):
+    return pl.pallas_call(
+        gather_kernel,
+        name="gather_weights",
+        out_shape=jax.ShapeDtypeStruct((6, NZ, 128, 128), jnp.bfloat16),
+        in_specs=[pl.BlockSpec(memory_space=pl.ANY)] * 6,
+        out_specs=pl.BlockSpec(memory_space=pltpu.VMEM),
+        scratch_shapes=[
+            pltpu.SemaphoreType.DMA((6,)),
+            pltpu.SemaphoreType.DMA((3,)),
+            pltpu.SemaphoreType.DMA((3,)),
+            pltpu.SemaphoreType.DMA((2, 3, 8)),
+            pltpu.SemaphoreType.DMA((2, 3, 8)),
+            pltpu.SemaphoreType.DMA((2, 8)),
+            pltpu.SemaphoreType.DMA((2, 8)),
+            pltpu.SemaphoreType.DMA((NZ, 3)),
+            pltpu.SemaphoreType.DMA((NZ, 3)),
+        ],
+        compiler_params=pltpu.CompilerParams(collective_id=0, has_side_effects=True),
+    )(*shards)
 
 
 def in_one_piece(arrays, axis, dim, along):
@@ -91,9 +221,9 @@
     features = tokens[0].astype(jnp.float32)
     mean_square = jnp.mean(features * features, axis=-1, keepdims=True)
     normed = (features * lax.rsqrt(mean_square + 1e-06) * norm_gain).astype(jnp.bfloat16)
-    weights = in_one_piece(
-        (w_state_in, w_value, w_outer, w_inner, w_state_out, w_conv_out), ("sp", "fs"), 0, 1
-    )
+    every_weight = gather_weights((w_state_in, w_value, w_state_out, w_inner, w_outer, w_conv_out))
+    every_weight = every_weight.reshape(6, 2048, 128)
+    weights = [every_weight[n] for n in (0, 1, 4, 3, 2, 5)]
 
     def project(matrix):
         return jnp.dot(normed, matrix, preferred_element_type=jnp.float32).astype(jnp.bfloat16)

time: 256 us -> 178 us (0.70)
  waiting for transfers between devices: 148 us -> 14.1 us
  Pallas kernels: 0 us -> 43.8 us
  local copies, waits for them, and re-layouts: 20.6 us -> 45.2 us
  between operations: 15.4 us -> 2.04 us
  other arithmetic: 14.3 us -> 20.9 us
  matrix products: 12.5 us -> 8.04 us
    all_gather x1 -> x0, waiting for transfers between devices: 134 us -> none  [in_one_piece(): lax.all_gather(both, axis, axis=dim, tiled=True)]
    pallas_call x0 -> x1, Pallas kernels: none -> 43.8 us  [gather_weights(): pl.pallas_call(gather_kernel, name='gather_weights', out_shape=jax.ShapeD...]
    slice x40, local copies, waits for them, and re-layouts: 0.67 us -> 24.8 us  [body(): running = lax.associative_scan(chain_pair, every, axis=0)]
    unnamed x45 -> x70, local copies, waits for them, and re-layouts: 5.2 us -> 1.47 us
    dot_general x3, matrix products: 5.03 us -> 1.59 us  [project(): jnp.dot(normed, matrix, preferred_element_type=jnp.float32)]
    slice x0 -> x1, local copies, waits for them, and re-layouts: none -> 3.19 us  [body(): weights = [every_weight[n] for n in (0, 1, 4, 3, 2, 5)]]
    all_to_all x1, starting transfers between devices: 21.2 us -> 18.5 us  [summed_on_arrival(): parts = lax.all_to_all(in_blocks(x, dim, length), axis, 0, 0, tiled=True)]
  transfers between devices with their start and end apart: 3 -> 2, of which waited for: 2 -> 1; matrix products, arithmetic and copies ran while one was open for 4% -> 36% of each run, Pallas kernels for 0% -> 0%
where the time goes in v1:
time: 178 us; the launch traced here: 176 us
  local copies, waits for them, and re-layouts  45.2 us (25%)
  Pallas kernels  43.8 us (25%)
  other arithmetic  20.9 us (12%)
  blocking collectives  20.9 us (12%)
  starting transfers between devices  20.7 us (12%)
  waiting for transfers between devices  14.1 us (8%)
  matrix products  8.04 us (5%)
  between operations  2.04 us (1%)
    pallas_call x1, Pallas kernels, gather_weights(): pl.pallas_call(gather_kernel, name='gather_weights', out_shape=jax.ShapeD...  43.8 us
    slice x40, local copies, waits for them, and re-layouts, body(): running = lax.associative_scan(chain_pair, every, axis=0)  24.8 us
    all_gather x1, blocking collectives, gather_together(): lines, at, done = (lax.all_gather(ravelled, axis), 0, [])  20.9 us
    all_to_all x1, starting transfers between devices, summed_on_arrival(): parts = lax.all_to_all(in_blocks(x, dim, length), axis, 0, 0, tiled=True)  18.5 us
    all_to_all x1, waiting for transfers between devices, summed_on_arrival(): parts = lax.all_to_all(in_blocks(x, dim, length), axis, 0, 0, tiled=True)  14.1 us
    another operation x1, other arithmetic, body(): jnp.stack([undo_real, undo_imag])  3.98 us
    reshape x2, local copies, waits for them, and re-layouts, body(): hidden_imag = (local_imag + shift_imag).reshape(rows, groups, states)  3.79 us
    sub x5, other arithmetic, complex_product(): left_real * right_real - left_imag * right_imag  3.62 us
  transfers between devices with their start and end apart: 2, of which 1 were waited for; matrix products, arithmetic and copies ran while one was open for 36% of the time, Pallas kernels for 0%

profile of v1, /device:TPU:1, one launch (start us, length us, event | category | flops | bytes accessed | tf_op | source)
XLA Modules:
  0.0 175.6 jit_solution(16282794231188551724)
XLA Ops:
  0.6 43.8 %gather_weights.1 = bf16[6,16,128,128]{3,2,1,0:T(8,128)(2,1)} custom-call(bf16[32,128]{1,0:T(8,128)(2,1)} %refs_0_.1, bf16[32,128]{1,0:T(8,128)(2,1)} %refs_1_.1, bf16[32,128]{1,0:T(8,128)(2,1)} %refs_2_.1, bf16[32,128]{1,0:T(8,128)(2,1)} %refs_3_.1, bf16[32,128]{1,0:T(8,128)(2,1)} %refs_4_.1, bf16[32,128]{1,0:T(8,128)(2,1)} %refs_5_.1), custom_call_target="tpu_custom_call" | custom-call | tf_op jit(solution)/shard_map/gather_weights/pallas_call | solution.py:118
  44.4 3.2 %fusion.75 = (bf16[1,16,128,128]{3,2,1,0:T(8,128)(2,1)S(1)}, bf16[1,16,128,128]{3,2,1,0:T(8,128)(2,1)}, bf16[1,16,128,128]{3,2,1,0:T(8,128)(2,1)S(1)}, bf16[1,16...) fusion(bf16[6,16,128,128]{3,2,1,0:T(8,128)(2,1)} %gather_weights.1), kind=kLoop, calls=%fused_computation.259 | loop fusion | bytes 6291456 | tf_op jit(solution)/shard_map/slice | solution.py:226
  49.6 2.2 %collective-permute-start = (bf16[2,128]{1,0:T(2,128)(2,1)}, bf16[2,128]{1,0:T(2,128)(2,1)}, u32[]{:S(2)}, u32[]{:S(2)}) collective-permute-start(bf16[2,128]{1,0:T(2,128)(2,1)} %slice.882), channel_id=1, source_target_pairs={{0,32},{32,64},{64,96},{96,128},{128,160},{160,192},{192,224},{224... | collective-permute-start | bytes 1544 | tf_op jit(solution)/shard_map/ppermute | solution.py:167
  52.4 0.7 convolution_bitcast_fusion
  53.7 1.1 reshape.240
  55.2 1.1 reshape.241
  57.5 2.0 %sine_bitcast_fusion = (f32[16,16,512]{2,0,1:T(8,128)S(1)}, f32[16,512,16]{1,0,2:T(8,128)S(1)}, f32[16,16,512]{2,0,1:T(8,128)S(1)}) fusion(f32[16,512,16]{1,2,0:T(8,128)S(1)} %fusion.52, f32[512]{0:T(512)S(1)} %mul.705, f32[512]{0:T(512)S(1)} %mul.698), kind=kLoop, calls=%fused_computation.44 | loop fusion | flops 262144 | bytes 2101248 | tf_op jit(solution)/shard_map/sin | solution.py:272
  59.6 4.0 %subtract_bitcast_fusion = (f32[1,16,16,512]{3,2,1,0:T(8,128)S(1)}, f32[1,16,16,512]{3,2,1,0:T(8,128)S(1)}, f32[16,16,512]{2,1,0:T(8,128)S(1)}) fusion(f32[16,512,16]{1,0,2:T(8,128)S(1)} %get-tuple-element.20, f32[16,512,16]{1,2,0:T(8,128)S(1)} %fusion.52, f32[512]{0:T(512)S(1)} %get-tuple-element.124, f32[16,16,512]{2,0,1:T(8,128)S(1)} %get-tuple-element.19, ...), kind=kLoop, calls=%fused_computation.42 | loop fusion | flops 3932160 | bytes 5251072 | tf_op jit(solution)/shard_map/stack | solution.py:277
  63.5 0.6 fusion.13
  64.2 0.6 copy.110
  64.8 1.5 multiply_subtract_fusion
  66.3 0.8 copy-done.1
  67.3 1.7 copy_add_fusion.1
  69.1 0.8 slice_bitcast_fusion.4
  71.1 0.6 multiply_subtract_fusion.4
  72.7 20.9 %all-gather = f32[32768]{0:T(1024)S(1)} all-gather(f32[2048]{0:T(1024)S(1)} %pad_maximum_fusion.12), channel_id=2, replica_groups=mesh['sp'=16,'fs'=4,'tp'=8] {'sp'}, dimensions={0}, use_global_device_ids=true | all-gather | bytes 139264 | tf_op jit(solution)/shard_map/all_gather | solution.py:156
  93.7 0.6 slice.676
  94.3 0.6 slice.677
  94.9 0.6 slice.679
  95.5 0.6 slice.680
  96.1 0.6 slice.713
  96.7 0.6 slice.716
  97.3 0.6 slice.715
  98.5 1.5 subtract_add_fusion.2
  100.0 1.3 slice.683
  101.3 1.3 slice.684
  103.2 0.6 slice.686
  103.9 1.3 slice.718
  105.2 1.3 slice.721
  106.5 1.3 slice.720
  107.8 1.3 slice.724
  109.1 1.4 multiply_subtract_fusion.7
  110.6 0.8 slice.689
  111.4 0.7 slice.690
  112.1 0.7 slice.691
  112.8 0.7 slice.692
  113.5 0.7 slice.723
  114.2 0.7 slice.726
  114.9 0.7 slice.725
  115.7 0.7 slice.728
  116.4 0.8 slice_add_fusion.17
  117.3 0.7 slice.682
  118.0 0.7 slice.739
  118.8 0.7 slice.742
  119.5 0.7 slice.859
  120.2 0.7 slice.878
  121.9 0.8 multiply_add_fusion.12
  122.7 0.7 slice.833
  124.0 0.7 pad_maximum_fusion.5
  124.7 0.7 pad_maximum_fusion.7
  125.4 0.7 fusion.79
  126.5 1.2 subtract_add_fusion
  128.0 1.2 reshape.242
  129.2 1.5 copy.75
  130.8 1.2 fusion.21
  132.0 2.3 %reshape.243 = f32[256,8,64]{2,1,0:T(8,128)} reshape(f32[16,16,512]{2,1,0:T(8,128)} %fusion.21) | data formatting | bytes 1048576 | tf_op jit(solution)/shard_map/reshape | solution.py:315
  134.3 1.5 copy.76
  135.9 1.2 fusion.34
  137.6 0.6 maximum_convert_fusion
  138.2 3.1 %fusion = bf16[256,2048]{1,0:T(8,128)(2,1)} fusion(f32[256,2048]{1,0:T(8,128)S(1)} %fusion.80, bf16[2048,128]{1,0:T(8,128)(2,1)} %bitcast.125, bf16[2048,128]{1,0:T(8,128)(2,1)} %bitcast.126, f32[258,128]{1,0:T(8,128)S(1)} %maximum_convert_fusion, f32[128]{0:T(128)S(1)} %get-tuple-element.121, f32[128]{0:T(128)S(1)} %get-tuple-element.122, ...), kind=kOutput, calls=%fused_computation.3 | convolution fusion | flops 271876096 | bytes 5646848 | tf_op jit(solution)/shard_map/rc,dc->rd/dot_general | solution.py:331
  141.3 18.5 %all-to-all-start = ((bf16[8,32,2048]{2,1,0:T(8,128)(2,1)}), bf16[8,32,2048]{2,1,0:T(8,128)(2,1)S(1)}, u32[]{:S(2)}, u32[]{:S(2)}) async-start(bf16[8,32,2048]{2,1,0:T(8,128)(2,1)} %bitcast.124), calls=%async_computation | async-start | bytes 2097152 | tf_op jit(solution)/shard_map/all_to_all | solution.py:177
  160.1 0.7 copy.77
  160.7 14.1 %all-to-all-done = bf16[8,32,2048]{2,1,0:T(8,128)(2,1)S(1)} async-done(((bf16[8,32,2048]{2,1,0:T(8,128)(2,1)}), bf16[8,32,2048]{2,1,0:T(8,128)(2,1)S(1)}, u32[]{:S(2)}, u32[]{:S(2)}) %all-to-all-start) | async-done | bytes 1048608 | tf_op jit(solution)/shard_map/all_to_all | solution.py:177
  174.8 0.8 reduce_sum.22
  (276 shorter events, 10.6 us)
Async XLA Ops:
  44.4 3.2 %copy-start = (bf16[1,256,2048]{2,1,0:T(8,128)(2,1)S(1)}, bf16[1,256,2048]{2,1,0:T(8,128)(2,1)}, u32[]{:S(2)}) copy-start(bf16[1,256,2048]{2,1,0:T(8,128)(2,1)} %param.19) | copy-start | bytes 3145732
  44.4 3.5 %copy-start.21 = (f32[2048]{0:T(1024)S(1)}, f32[2048]{0:T(1024)}, u32[]{:S(2)}) copy-start(f32[2048]{0:T(1024)} %param.20) | copy-start | bytes 24580
  47.9 3.9 %copy-start.24 = (f32[256]{0:T(256)}, f32[256]{0:T(256)S(1)}, u32[]{:S(2)}) copy-start(f32[256]{0:T(256)S(1)} %add_rsqrt_fusion) | copy-start | bytes 3076
  48.4 3.9 %copy-start.14 = (f32[8,64,16]{1,2,0:T(8,128)S(1)}, f32[8,64,16]{1,2,0:T(8,128)}, u32[]{:S(2)}) copy-start(f32[8,64,16]{1,2,0:T(8,128)} %param.32) | copy-start | bytes 98308
  48.4 3.9 %copy-start.15 = (f32[8,64,16]{1,2,0:T(8,128)S(1)}, f32[8,64,16]{1,2,0:T(8,128)}, u32[]{:S(2)}) copy-start(f32[8,64,16]{1,2,0:T(8,128)} %param.31) | copy-start | bytes 98308
  49.0 2.8 %copy-start.17 = (bf16[256,128]{1,0:T(8,128)(2,1)}, bf16[256,128]{1,0:T(8,128)(2,1)S(1)}, u32[]{:S(2)}) copy-start(bf16[256,128]{1,0:T(8,128)(2,1)S(1)} %fusion.7) | copy-start | bytes 196612
  49.6 88.0 %collective-permute-start = (bf16[2,128]{1,0:T(2,128)(2,1)}, bf16[2,128]{1,0:T(2,128)(2,1)}, u32[]{:S(2)}, u32[]{:S(2)}) collective-permute-start(bf16[2,128]{1,0:T(2,128)(2,1)} %slice.882), channel_id=1, source_target_pairs={{0,32},{32,64},{64,96},{96,128},{128,160},{160,192},{192,224},{224... | collective-permute-start | bytes 1544 | tf_op jit(solution)/shard_map/ppermute | solution.py:167
  53.6 2.6 %copy-start.30 = (f32[8]{0:T(128)S(1)}, f32[8]{0:T(128)}, u32[]{:S(2)}) copy-start(f32[8]{0:T(128)} %param.27) | copy-start | bytes 100
  53.7 2.6 %copy-start.29 = (f32[1,256]{1,0:T(1,128)S(1)}, f32[1,256]{1,0:T(1,128)}, u32[]{:S(2)}) copy-start(f32[1,256]{1,0:T(1,128)} %param.30) | copy-start | bytes 3076
  56.2 1.1 copy-start.26
  56.2 1.2 copy-start.27
  57.0 2.6 %copy-start.5 = (f32[16,16,512]{2,1,0:T(8,128)S(1)}, f32[16,16,512]{2,1,0:T(8,128)}, u32[]{:S(2)}) copy-start(f32[16,16,512]{2,1,0:T(8,128)} %reshape.240) | copy-start | bytes 1572868
  66.3 0.8 copy-start.1
  67.3 3.2 %copy-start.2 = (f32[16,16,512]{2,0,1:T(8,128)S(1)}, f32[16,16,512]{2,0,1:T(8,128)}, u32[]{:S(2)}) copy-start(f32[16,16,512]{2,0,1:T(8,128)} %copy-done.1) | copy-start | bytes 1572868
  69.0 40.2 %copy-start.3 = (f32[16,16,512]{2,1,0:T(8,128)}, f32[16,16,512]{2,1,0:T(8,128)S(1)}, u32[]{:S(2)}) copy-start(f32[16,16,512]{2,1,0:T(8,128)S(1)} %copy_add_fusion.1) | copy-start | bytes 1572868
  71.0 1.2 copy-start.8
  72.0 0.6 copy-start.12
  72.1 0.6 copy-start.10
  110.6 15.7 %copy-start.13 = (f32[16,512]{1,0:T(8,128)S(1)}, f32[16,512]{1,0:T(8,128)}, u32[]{:S(2)}) copy-start(f32[16,512]{1,0:T(8,128)} %copy-done.12) | copy-start | bytes 98308
  110.6 15.7 %copy-start.20 = (f32[7,512]{1,0:T(8,128)S(1)}, f32[7,512]{1,0:T(8,128)}, u32[]{:S(2)}) copy-start(f32[7,512]{1,0:T(8,128)} %get-tuple-element.40) | copy-start | bytes 43012
  110.6 15.7 %copy-start.9 = (f32[16,512]{1,0:T(8,128)S(1)}, f32[16,512]{1,0:T(8,128)}, u32[]{:S(2)}) copy-start(f32[16,512]{1,0:T(8,128)} %copy-done.8) | copy-start | bytes 98308
  110.6 15.7 %copy-start.11 = (f32[16,512]{1,0:T(8,128)S(1)}, f32[16,512]{1,0:T(8,128)}, u32[]{:S(2)}) copy-start(f32[16,512]{1,0:T(8,128)} %copy-done.10) | copy-start | bytes 98308
  128.0 2.7 %copy-start.4 = (f32[16,16,512]{2,1,0:T(8,128)S(1)}, f32[16,16,512]{2,1,0:T(8,128)}, u32[]{:S(2)}) copy-start(f32[16,16,512]{2,1,0:T(8,128)} %copy-done.3) | copy-start | bytes 1572868
  129.2 1.5 copy-start.7
  132.0 3.8 %copy-start.19 = (f32[8,16,64]{2,1,0:T(8,128)S(1)}, f32[8,16,64]{2,1,0:T(8,128)}, u32[]{:S(2)}) copy-start(f32[8,16,64]{2,1,0:T(8,128)} %param.34) | copy-start | bytes 98308
  132.0 3.8 %copy-start.16 = (f32[8,16,64]{2,1,0:T(8,128)S(1)}, f32[8,16,64]{2,1,0:T(8,128)}, u32[]{:S(2)}) copy-start(f32[8,16,64]{2,1,0:T(8,128)} %param.33) | copy-start | bytes 98308
  132.0 3.8 %copy-start.23 = (f32[8,16]{1,0:T(8,128)S(1)}, f32[8,16]{1,0:T(8,128)}, u32[]{:S(2)}) copy-start(f32[8,16]{1,0:T(8,128)} %param.35) | copy-start | bytes 1540
  134.3 2.8 %copy-start.6 = (bf16[1,16,128,128]{3,2,1,0:T(8,128)(2,1)S(1)}, bf16[1,16,128,128]{3,2,1,0:T(8,128)(2,1)}, u32[]{:S(2)}) copy-start(bf16[1,16,128,128]{3,2,1,0:T(8,128)(2,1)} %get-tuple-element.12) | copy-start | bytes 1572868
  135.8 1.7 copy-start.28
  135.8 1.7 copy-start.18
  135.8 2.4 %copy-start.22 = (f32[2048]{0:T(1024)S(1)}, f32[2048]{0:T(1024)}, u32[]{:S(2)}) copy-start(f32[2048]{0:T(1024)} %param.20) | copy-start | bytes 24580
  135.9 2.4 %copy-start.25 = (f32[256]{0:T(256)S(1)}, f32[256]{0:T(256)}, u32[]{:S(2)}) copy-start(f32[256]{0:T(256)} %copy-done.24) | copy-start | bytes 3076
  141.3 33.5 %all-to-all-start = ((bf16[8,32,2048]{2,1,0:T(8,128)(2,1)}), bf16[8,32,2048]{2,1,0:T(8,128)(2,1)S(1)}, u32[]{:S(2)}, u32[]{:S(2)}) async-start(bf16[8,32,2048]{2,1,0:T(8,128)(2,1)} %bitcast.124), calls=%async_computation | async-start | bytes 2097152 | tf_op jit(solution)/shard_map/all_to_all | solution.py:177

commit v2 on v1

v2 whole, which is shorter than its diff:
```python
import math

import jax
import jax.numpy as jnp
from jax import lax
from jax.experimental import pallas as pl
from jax.experimental.pallas import tpu as pltpu
from jax.sharding import PartitionSpec as P

MESH = pl.DeviceIdType.MESH
HIGHEST = lax.Precision.HIGHEST
F32, BF16 = jnp.float32, jnp.bfloat16
NZ, NY, NX = 16, 4, 4
ROWS, D, CH, FLAT = 256, 2048, 128, 512
NT = (((1,), (1,)), ((), ()))
NCHUNK = 4
CW = D // NCHUNK
SIN = [math.pi, -(math.pi**3) / 6, math.pi**5 / 120, -(math.pi**7) / 5040, math.pi**9 / 362880, -(math.pi**11) / 39916800]
COS = [1.0, -(math.pi**2) / 2, math.pi**4 / 24, -(math.pi**6) / 720, math.pi**8 / 40320, -(math.pi**10) / 3628800, math.pi**12 / 479001600]


def horner(coefs, x):
    total = jnp.full_like(x, coefs[-1])
    for c in coefs[-2::-1]:
        total = total * x + c
    return total


def complex_power(rate, turn, fall):
    u = rate * turn
    r = u - jnp.round(u)
    x = r * r
    s = r * horner(SIN, x)
    c = horner(COS, x)
    grow = jnp.exp2(rate * fall)
    return grow * (1.0 - 2.0 * (s * s)), grow * (2.0 * (s * c))


def iota(shape, dim):
    return lax.broadcasted_iota(jnp.int32, shape, dim)


def lanes4(x):
    return jnp.concatenate([x, x, x, x], axis=1)


def layer_kernel(*refs):
    n_small = 12
    tokens = refs[0]
    shards = refs[1:7]
    small = refs[7 : 7 + n_small]
    out, fin = refs[7 + n_small : 9 + n_small]
    rest = refs[9 + n_small :]
    small_v = rest[:n_small]
    (
        wg, tk, nb, prm, pk, ratep, tchunk, ring_t, br, bi, pc, dr, di, coup, readw, xp_s, ext, halo,
        ends, ec, hc, rows8, hd, mix, ps, pr, cs, rb,
        ssem, lsem, tsem, ya_s, ya_r, az_s, az_r, bz_s, bz_r, by_s, by_r, tz_s, tz_r, h_s, h_r, e_s, e_r,
        p_s, p_r, x_s, x_r,
    ) = rest[n_small:]
    gain, lstep, decay, freq, rate, in_r, in_i, rd_r, rd_i, skip, taps, init = small_v
    z = lax.axis_index("sp")
    y = lax.axis_index("fs")
    t = lax.axis_index("tp")
    xx, cc = t // 2, lax.rem(t, 2)
    other = 1 - cc
    zn, zp = lax.rem(z + 1, NZ), lax.rem(z + NZ - 1, NZ)

    loads = [pltpu.make_async_copy(s, v, ssem.at[n]) for n, (s, v) in enumerate(zip(small, small_v))]
    mine = pl.ds(pl.multiple_of(z * 128 + y * 32, 32), 32)
    local = [pltpu.make_async_copy(shards[w], wg.at[w, mine, :], lsem.at[w]) for w in range(6)]
    tok = pltpu.make_async_copy(tokens, tk, tsem)
    for c in local:
        c.start()
    for c in loads:
        c.start()
    tok.start()

    barrier = pltpu.get_barrier_semaphore()
    for d in range(1, NY):
        pl.semaphore_signal(barrier, inc=1, device_id=(z, lax.rem(y + d, NY), t), device_id_type=MESH)
    for n in (zn, zp):
        pl.semaphore_signal(barrier, inc=1, device_id=(n, y, t), device_id_type=MESH)
    for d in range(1, NX):
        pl.semaphore_signal(barrier, inc=1, device_id=(z, y, lax.rem(xx + d, NX) * 2 + cc), device_id_type=MESH)
    pl.semaphore_signal(barrier, inc=1, device_id=(z, y, xx * 2 + other), device_id_type=MESH)
    pl.semaphore_wait(barrier, 9)
    for c in local:
        c.wait()

    def a_y(d):
        return pltpu.make_async_remote_copy(
            wg.at[pl.ds(0, 3), mine, :], wg.at[pl.ds(0, 3), mine, :], ya_s.at[d - 1], ya_r.at[d - 1],
            device_id=(z, lax.rem(y + d, NY), t), device_id_type=MESH)

    def b_rows(zb):
        return pl.ds(pl.multiple_of(zb * 128 + y * 32, 32), 32)

    def b_y(k, d):
        zb = lax.rem(z + k + NZ, NZ)
        return pltpu.make_async_remote_copy(
            wg.at[pl.ds(3, 3), b_rows(zb), :], wg.at[pl.ds(3, 3), b_rows(zb), :], by_s.at[zb, d - 1], by_r.at[zb, d - 1],
            device_id=(z, lax.rem(y + d, NY), t), device_id_type=MESH)

    def b_z(k, side):
        zb = lax.rem(z + (k if side else NZ - k), NZ)
        return pltpu.make_async_remote_copy(
            wg.at[pl.ds(3, 3), b_rows(zb), :], wg.at[pl.ds(3, 3), b_rows(zb), :], bz_s.at[side, k], bz_r.at[side, k],
            device_id=(zp if side else zn, y, t), device_id_type=MESH)

    def a_z(k, side, w):
        zb = lax.rem(z + (k if side else NZ - k), NZ)
        rows = pl.ds(pl.multiple_of(zb * 128, 128), 128)
        return pltpu.make_async_remote_copy(
            wg.at[w, rows, :], wg.at[w, rows, :], az_s.at[side, w, k], az_r.at[side, w, k],
            device_id=(zp if side else zn, y, t), device_id_type=MESH)

    def t_z(k, side):
        zb = lax.rem(z + (k if side else NZ - k), NZ)
        return pltpu.make_async_remote_copy(
            ring_t.at[zb], ring_t.at[zb], tz_s.at[side, k], tz_r.at[side, k],
            device_id=(zp if side else zn, y, t), device_id_type=MESH)

    for d in (2, 1, 3):
        a_y(d).start()
    for side in (0, 1):
        b_z(0, side).start()
    for d in (2, 1, 3):
        b_y(0, d).start()

    for c in loads:
        c.wait()
    row, col = iota((ROWS, ROWS), 0), iota((ROWS, ROWS), 1)
    interleave = col == (row & 7) * 32 + (row >> 3)
    spread = jnp.where(interleave, rate[...], 0.0)
    ratep[...] = jnp.dot(spread, jnp.ones((ROWS, 128), F32), precision=HIGHEST, preferred_element_type=F32)
    totals = jnp.sum(ratep[...].reshape(32, 8, 128), axis=0)
    tchunk[...] = totals
    ring_t[z] = jnp.sum(totals, axis=0, keepdims=True)

    for d in (1, 3, 2):
        a_y(d).wait_recv()
    for w in range(3):
        for side in (0, 1):
            a_z(0, side, w).start()
    for side in (0, 1):
        t_z(0, side).start()

    tall = jnp.concatenate([decay[...], freq[...], init[...]], axis=0)
    hot = ((iota((64, FLAT), 1) & 63) == iota((64, FLAT), 0)).astype(F32)
    wide = jnp.dot(tall, hot, precision=HIGHEST, preferred_element_type=F32)
    own = (iota((8, FLAT), 1) >> 6) == iota((8, FLAT), 0)

    def line(v):
        return jnp.sum(jnp.where(own, v, 0.0), axis=0, keepdims=True)

    decay_l, freq_l = line(wide[0:8]), line(wide[8:16])
    dt = jnp.exp(line(jnp.broadcast_to(lstep[...], (8, FLAT))))
    modulus = decay_l * decay_l + freq_l * freq_l
    lines = [dt * freq_l * (0.5 / math.pi), dt * decay_l * math.log2(math.e), decay_l / modulus, -freq_l / modulus,
             line(wide[16:24]), line(wide[24:32])]
    for n, v in enumerate(lines):
        prm[n : n + 1, :] = v
        for i in range(4):
            pk[n, i : i + 1, :] = v[:, i * 128 : (i + 1) * 128]
    c_re, c_im = complex_power(lanes4(tchunk[...]), prm[0:1, :], prm[1:2, :])
    pc[0] = c_re
    pc[1] = c_im
    hot16 = ((iota((16, CH), 1) & 15) == iota((16, CH), 0)).astype(BF16)
    block = (iota((FLAT, CH), 0) >> 6) == (iota((FLAT, CH), 1) >> 4)
    for n, src in enumerate((in_r, in_i)):
        w = jnp.dot(src[...].astype(BF16), hot16, preferred_element_type=F32)
        coup[n * FLAT : (n + 1) * FLAT, :] = jnp.where(block, w, 0.0).astype(BF16)
    block_t = (iota((CH, FLAT), 1) >> 6) == (iota((CH, FLAT), 0) >> 4)
    hot64 = hot.astype(BF16)
    for n, src in enumerate((rd_r, rd_i)):
        w = jnp.dot(src[...].astype(BF16), hot64, preferred_element_type=F32)
        readw[:, n * FLAT : (n + 1) * FLAT] = jnp.where(block_t, w if n == 0 else -w, 0.0).astype(BF16)
    tok.wait()

    def work(k):
        rows = pl.ds(pl.multiple_of((k - 1) * 32, 32), 32)
        f = tk[rows, :].astype(F32)
        mean_square = jnp.mean(f * f, axis=-1, keepdims=True)
        nb[rows, :] = (f * lax.rsqrt(mean_square + 1e-06) * gain[...]).astype(BF16)
        for half in range(2):
            rows = pl.ds(pl.multiple_of((k - 1) * 32 + half * 16, 16), 16)
            re, im = complex_power(lanes4(ratep[rows, :]), prm[0:1, :], prm[1:2, :])
            br[rows, :] = re
            bi[rows, :] = im

    def step(k, right, left):
        sides = [s for s, on in ((0, right), (1, left)) if on is not None]
        fwd = {0: right, 1: left}
        for s in sides:
            b_z(k - 1, s).wait_recv()
            if fwd[s]:
                b_z(k, s).start()
            for d in (2, 1, 3):
                b_y(k if s else -k, d).start()
        for w in range(3):
            for s in sides:
                a_z(k - 1, s, w).wait_recv()
                if fwd[s]:
                    a_z(k, s, w).start()
        for s in sides:
            t_z(k - 1, s).wait_recv()
            if fwd[s]:
                t_z(k, s).start()
        work(k)

    def loop(k, c):
        step(k, True, True)
        return c

    lax.fori_loop(1, 7, loop, 0)
    step(7, True, False)
    step(8, False, None)

    def drain_y(k, c):
        for d in (1, 2, 3):
            b_y(k, d).wait_recv()
        return c

    def project(w):
        return jnp.dot(nb[...], wg[w], preferred_element_type=F32).astype(BF16)

    state_in = project(0)
    value = project(1).astype(F32)
    lax.fori_loop(0, NZ, drain_y, 0)
    inner = project(3).astype(F32)
    gated = (inner * value).astype(BF16).astype(F32)
    ext[8 : 8 + ROWS, :] = gated

    perm = jnp.where(interleave, 1.0, 0.0).astype(BF16)
    xp = jnp.dot(perm, state_in, preferred_element_type=F32)
    xp_s[...] = xp
    drive = lax.dot_general(xp.astype(BF16), coup[...], NT, preferred_element_type=F32)
    v_re, v_im = drive[:, :FLAT], drive[:, FLAT:]
    a_re, a_im = prm[2:3, :], prm[3:4, :]
    dr[...] = v_re * a_re - v_im * a_im
    di[...] = v_re * a_im + v_im * a_re
    h_copy = pltpu.make_async_remote_copy(
        ext.at[pl.ds(ROWS, 8), :], halo, h_s, h_r, device_id=(zn, y, t), device_id_type=MESH)
    h_copy.start()

    def advance(j, h):
        rows = pl.ds(pl.multiple_of(j * 8, 8), 8)
        b_re, b_im, d_re, d_im = br[rows, :], bi[rows, :], dr[rows, :], di[rows, :]
        re, im = h[0] + d_re, h[1] + d_im
        return (b_re * re - b_im * im - d_re, b_re * im + b_im * re - d_im)

    zero = jnp.zeros((8, FLAT), F32)
    end_re, end_im = lax.fori_loop(0, 32, advance, (zero, zero))
    ec[0] = end_re
    ec[1] = end_im

    def chain(re, im, keep):
        for c in range(8):
            if keep:
                hc[0, c : c + 1, :] = re
                hc[1, c : c + 1, :] = im
            p_re, p_im = pc[0, c : c + 1, :], pc[1, c : c + 1, :]
            re, im = (p_re * re - p_im * im + ec[0, c : c + 1, :], p_re * im + p_im * re + ec[1, c : c + 1, :])
        return re, im

    none = jnp.zeros((1, FLAT), F32)
    e_re, e_im = chain(none, none, False)
    for i in range(4):
        ends[z, i : i + 1, :] = e_re[:, i * 128 : (i + 1) * 128]
        ends[z, 4 + i : 5 + i, :] = e_im[:, i * 128 : (i + 1) * 128]

    outer = project(4).astype(F32)

    def e_copy(d):
        return pltpu.make_async_remote_copy(
            ends.at[z], ends.at[z], e_s.at[d - 1], e_r.at[d - 1],
            device_id=(lax.rem(z + d, NZ), y, t), device_id_type=MESH)

    for d in (8, 7, 9, 6, 10, 5, 11, 4, 12, 3, 13, 2, 14, 1, 15):
        e_copy(d).start()
    h_copy.wait_recv()
    ext[0:8, :] = jnp.where(z == 0, 0.0, halo[...])
    filtered = taps[0:1, :] * ext[6 : 6 + ROWS, :] + taps[1:2, :] * ext[7 : 7 + ROWS, :] + taps[2:3, :] * ext[8 : 8 + ROWS, :]
    mix[:, CH:] = (outer * filtered).astype(BF16)

    def span_power(j):
        return complex_power(ring_t[j], pk[0, 0:4, :], pk[1, 0:4, :])

    powers = [span_power(j) for j in range(NZ)]
    for d in range(1, NZ):
        e_copy(d).wait_recv()
    re, im = pk[4, 0:4, :], pk[5, 0:4, :]
    in_re, in_im = re, im
    for j in range(NZ):
        p_re, p_im = powers[j]
        re, im = (p_re * re - p_im * im + ends[j, 0:4, :], p_re * im + p_im * re + ends[j, 4:8, :])
        if j < NZ - 1:
            here = z == j + 1
            in_re, in_im = jnp.where(here, re, in_re), jnp.where(here, im, in_im)
    rows8[0, 0:4, :] = in_re
    rows8[0, 4:8, :] = in_im
    rows8[1, 0:4, :] = re
    rows8[1, 4:8, :] = im

    def as_line(n, at):
        return jnp.concatenate([rows8[n, at + i : at + i + 1, :] for i in range(4)], axis=1)

    chain(as_line(0, 0), as_line(0, 4), True)

    def advance2(i, h):
        one = advance(2 * i, h)
        two = advance(2 * i + 1, one)
        rows = pl.ds(pl.multiple_of(i * 16, 16), 16)
        hd[rows, :FLAT] = jnp.concatenate([one[0], two[0]], axis=0).astype(BF16)
        hd[rows, FLAT:] = jnp.concatenate([one[1], two[1]], axis=0).astype(BF16)
        return two

    lax.fori_loop(0, 16, advance2, (hc[0], hc[1]))
    skip_w = jnp.dot(skip[...], ((iota((16, CH), 1) & 15) == iota((16, CH), 0)).astype(F32), precision=HIGHEST, preferred_element_type=F32)
    skip_l = jnp.sum(jnp.where((iota((8, CH), 1) >> 4) == iota((8, CH), 0), skip_w, 0.0), axis=0, keepdims=True)
    v = lax.dot_general(hd[...], readw[...], NT, preferred_element_type=F32) + skip_l * xp_s[...]
    smix = (0.5 * v * (1.0 + jnp.tanh(0.7978845608028654 * (v + 0.044715 * (v * v * v))))).astype(BF16)
    back = jnp.where(col == (row & 31) * 8 + (row >> 5), 1.0, 0.0).astype(BF16)
    mix[:, :CH] = jnp.dot(back, smix, preferred_element_type=F32).astype(BF16)

    def rows_of(core):
        return jnp.concatenate([mix[pl.ds(pl.multiple_of(b * 64 + core * 32, 32), 32), :] for b in range(NX)], axis=0)

    def w_out(n):
        return jnp.concatenate([wg[2, n * CW : (n + 1) * CW, :], wg[5, n * CW : (n + 1) * CW, :]], axis=1)

    def p_copy(n):
        return pltpu.make_async_remote_copy(
            ps.at[n], pr.at[n], p_s.at[n], p_r.at[n], device_id=(z, y, xx * 2 + other), device_id_type=MESH)

    def x_copy(n, d):
        to = lax.rem(xx + d, NX)
        return pltpu.make_async_remote_copy(
            cs.at[n, to], rb.at[n, d - 1], x_s.at[n, d - 1], x_r.at[n, d - 1],
            device_id=(z, y, to * 2 + cc), device_id_type=MESH)

    theirs, ours = rows_of(other), rows_of(cc)
    for n in range(NCHUNK):
        ps[n] = lax.dot_general(theirs, w_out(n), NT, preferred_element_type=F32).astype(BF16)
        p_copy(n).start()
    for n in range(NCHUNK):
        part = lax.dot_general(ours, w_out(n), NT, preferred_element_type=F32)
        p_copy(n).wait_recv()
        cs[n] = (part + pr[n].astype(F32)).astype(BF16).reshape(NX, 32, CW)
        for d in (2, 1, 3):
            x_copy(n, d).start()
    far = jnp.where(own, jnp.broadcast_to(as_line(1, 0), (8, FLAT)), 0.0)
    far_i = jnp.where(own, jnp.broadcast_to(as_line(1, 4), (8, FLAT)), 0.0)
    pick = ((iota((FLAT, 4), 0) & 63) == z * 4 + iota((FLAT, 4), 1)).astype(F32)
    fin[0] = jnp.dot(far, pick, precision=HIGHEST, preferred_element_type=F32)
    fin[1] = jnp.dot(far_i, pick, precision=HIGHEST, preferred_element_type=F32)
    for n in range(NCHUNK):
        for d in (1, 3, 2):
            x_copy(n, d).wait_recv()
        total = cs[n, xx].astype(F32) + rb[n, 0].astype(F32) + rb[n, 1].astype(F32) + rb[n, 2].astype(F32)
        out[:, n * CW : (n + 1) * CW] = total.astype(BF16)

    for d in (1, 2, 3):
        a_y(d).wait_send()

    def drain_send(k, c):
        for d in (1, 2, 3):
            b_y(k, d).wait_send()
        return c

    lax.fori_loop(0, NZ, drain_send, 0)

    def drain(k, c):
        for s in (0, 1):
            b_z(k, s).wait_send()
            t_z(k, s).wait_send()
            for w in range(3):
                a_z(k, s, w).wait_send()
        return c

    lax.fori_loop(0, 7, drain, 0)
    b_z(7, 0).wait_send()
    t_z(7, 0).wait_send()
    for w in range(3):
        a_z(7, 0, w).wait_send()
    h_copy.wait_send()
    for d in range(1, NZ):
        e_copy(d).wait_send()
    for n in range(NCHUNK):
        p_copy(n).wait_send()
        for d in (1, 2, 3):
            x_copy(n, d).wait_send()


def body(
    tokens, norm_gain, w_state_in, w_value, w_outer, w_inner, w_state_out, w_conv_out, log_step, decay_real, frequency,
    step_rate, input_real, input_imag, read_real, read_imag, skip_gain, conv_taps, initial_state,
):
    small = (
        norm_gain.reshape(1, D), log_step.reshape(8, 1), decay_real, frequency, step_rate, input_real.reshape(FLAT, 16),
        input_imag.reshape(FLAT, 16), read_real.reshape(CH, 64), read_imag.reshape(CH, 64), skip_gain, conv_taps,
        initial_state.reshape(16, 64),
    )
    dma = pltpu.SemaphoreType.DMA
    anywhere = pl.BlockSpec(memory_space=pl.ANY)
    vmem = pl.BlockSpec(memory_space=pltpu.VMEM)
    mixed, final = pl.pallas_call(
        layer_kernel,
        name="layer",
        out_shape=(jax.ShapeDtypeStruct((32, D), BF16), jax.ShapeDtypeStruct((2, 8, 4), F32)),
        in_specs=[anywhere] * (7 + len(small)),
        out_specs=(vmem, vmem),
        scratch_shapes=[pltpu.VMEM(a.shape, a.dtype) for a in small]
        + [
            pltpu.VMEM((6, D, CH), BF16),
            pltpu.VMEM((ROWS, D), BF16),
            pltpu.VMEM((ROWS, D), BF16),
            pltpu.VMEM((8, FLAT), F32),
            pltpu.VMEM((6, 8, 128), F32),
            pltpu.VMEM((ROWS, 128), F32),
            pltpu.VMEM((8, 128), F32),
            pltpu.VMEM((NZ, 1, 128), F32),
            pltpu.VMEM((ROWS, FLAT), F32),
            pltpu.VMEM((ROWS, FLAT), F32),
            pltpu.VMEM((2, 8, FLAT), F32),
            pltpu.VMEM((ROWS, FLAT), F32),
            pltpu.VMEM((ROWS, FLAT), F32),
            pltpu.VMEM((2 * FLAT, CH), BF16),
            pltpu.VMEM((CH, 2 * FLAT), BF16),
            pltpu.VMEM((ROWS, CH), F32),
            pltpu.VMEM((8 + ROWS, CH), F32),
            pltpu.VMEM((8, CH), F32),
            pltpu.VMEM((NZ, 8, 128), F32),
            pltpu.VMEM((2, 8, FLAT), F32),
            pltpu.VMEM((2, 8, FLAT), F32),
            pltpu.VMEM((2, 8, 128), F32),
            pltpu.VMEM((ROWS, 2 * FLAT), BF16),
            pltpu.VMEM((ROWS, 2 * CH), BF16),
            pltpu.VMEM((NCHUNK, 128, CW), BF16),
            pltpu.VMEM((NCHUNK, 128, CW), BF16),
            pltpu.VMEM((NCHUNK, NX, 32, CW), BF16),
            pltpu.VMEM((NCHUNK, NX - 1, 32, CW), BF16),
            dma((len(small),)),
            dma((6,)),
            dma,
            dma((3,)), dma((3,)),
            dma((2, 3, 8)), dma((2, 3, 8)),
            dma((2, 8)), dma((2, 8)),
            dma((NZ, 3)), dma((NZ, 3)),
            dma((2, 8)), dma((2, 8)),
            dma, dma,
            dma((NZ - 1,)), dma((NZ - 1,)),
            dma((NCHUNK,)), dma((NCHUNK,)),
            dma((NCHUNK, 3)), dma((NCHUNK, 3)),
        ],
        compiler_params=pltpu.CompilerParams(collective_id=0, has_side_effects=True),
    )(tokens.reshape(ROWS, D), w_state_in, w_value, w_state_out, w_inner, w_outer, w_conv_out, *small)
    return (mixed.reshape(1, 32, D), final.reshape(1, 2, 8, 4))


def solution(mesh):
    return jax.shard_map(
        body,
        mesh=mesh,
        in_specs=(
            P("fs", "sp", None),
            P(),
            P(("sp", "fs"), "tp"),
            P(("sp", "fs"), "tp"),
            P(("sp", "fs"), "tp"),
            P(("sp", "fs"), "tp"),
            P(("sp", "fs"), "tp"),
            P(("sp", "fs"), "tp"),
            P("tp"),
            P("tp", None),
            P("tp", None),
            P("fs", "sp"),
            P("tp", None, None),
            P("tp", None, None),
            P("tp", None, None),
            P("tp", None, None),
            P("tp", None),
            P(None, "tp"),
            P("fs", None, "tp", None),
        ),
        out_specs=(P("fs", ("sp", "tp"), None), P("fs", None, "tp", "sp")),
        check_vma=False,
    )
```

time: 178 us -> 78.8 us (0.44); the launches traced: 176 us -> 78.5 us
  local copies, waits for them, and re-layouts: 45.2 us -> 6.79 us
  Pallas kernels: 43.8 us -> 71.1 us
  other arithmetic: 20.9 us -> 0 us
  blocking collectives: 20.9 us -> 0 us
  starting transfers between devices: 20.7 us -> 0 us
  waiting for transfers between devices: 14.1 us -> 0 us
  matrix products: 8.04 us -> 0 us
    slice x94 -> x0, local copies, waits for them, and re-layouts: 31 us -> none  [the longest x40 24.8 us: body(): running = lax.associative_scan(chain_pair, every, axis=0)]
    pallas_call x1, Pallas kernels: 43.8 us -> 71.1 us  [body(): pl.pallas_call(layer_kernel, name='layer', out_shape=(jax.ShapeDtypeStruc...]
    all_gather x1 -> x0, blocking collectives: 20.9 us -> none  [gather_together(): lines, at, done = (lax.all_gather(ravelled, axis), 0, [])]
    all_to_all x1 -> x0, starting transfers between devices: 18.5 us -> none  [summed_on_arrival(): parts = lax.all_to_all(in_blocks(x, dim, length), axis, 0, 0, tiled=True)]
    all_to_all x1 -> x0, waiting for transfers between devices: 14.1 us -> none  [summed_on_arrival(): parts = lax.all_to_all(in_blocks(x, dim, length), axis, 0, 0, tiled=True)]
    dot_general x9 -> x0, matrix products: 8.04 us -> none  [the longest x1 3.06 us: body(): jnp.einsum('rc,dc->rd', conv_mix, weights[5], preferred_element_type=jnp....]
    reshape x6 -> x1, local copies, waits for them, and re-layouts: 8.65 us -> 0.67 us  [body(): log_step.reshape(8, 1)]
    add x53 -> x0, other arithmetic: 7.69 us -> none  [the longest x6 2.53 us: complex_product(): left_real * right_imag + left_imag * right_real]
  transfers between devices with their start and end apart: 2 -> 0, of which waited for: 1 -> 0; matrix products, arithmetic and copies ran while one was open for 36% -> 0% of each run, Pallas kernels for 0% -> 0%
where the time goes in v2:
time: 78.8 us; the launch traced here: 78.5 us
  Pallas kernels  71.1 us (90%)
  local copies, waits for them, and re-layouts  6.79 us (9%)
    pallas_call x1, Pallas kernels, body(): pl.pallas_call(layer_kernel, name='layer', out_shape=(jax.ShapeDtypeStruc...  71.1 us
    unnamed x7, local copies, waits for them, and re-layouts  4.75 us

profile of v2, /device:TPU:1, one launch (start us, length us, event | category | flops | bytes accessed | tf_op | source)
XLA Modules:
  0.0 78.5 jit_solution(11574138200079245870)
XLA Ops:
  0.6 0.0 copy-start.1
  0.6 0.6 copy-done.1
  1.3 0.7 copy.23.refs_8_
  2.0 0.0 copy-start
  2.0 1.7 %copy.21 = f32[8,64,16]{2,1,0:T(8,128)} copy(f32[8,64,16]{1,2,0:T(8,128)} %param.31) | data formatting | bytes 65536 | tf_op args[12]
  3.7 0.0 copy-done
  3.7 0.8 %copy.22 = f32[8,64,16]{2,1,0:T(8,128)} copy(f32[8,64,16]{1,2,0:T(8,128)S(1)} %copy-done) | data formatting | bytes 65536 | tf_op args[13]
  4.5 71.1 %layer.1 = (bf16[32,2048]{1,0:T(8,128)(2,1)}, f32[2,8,4]{2,1,0:T(8,128)}) custom-call(bf16[256,2048]{1,0:T(8,128)(2,1)} %bitcast.10, bf16[32,128]{1,0:T(8,128)(2,1)} %refs_1_.1, bf16[32,128]{1,0:T(8,128)(2,1)} %refs_2_.1, bf16[32,128]{1,0:T(8,128)(2,1)} %refs_3_.1, bf16[32,128]{1,0:T(8,128)(2,1)} %refs_4_.1, bf16[32,128]{1,0:T(8,128)(2,1)} %refs_5_.1, ...), custom_call_target="tpu_custom_call" | custom-call | tf_op jit(solution)/shard_map/layer/pallas_call | solution.py:408
  75.6 1.4 %copy.24 = f32[2,8,4]{1,2,0:T(4,128)} copy(f32[2,8,4]{2,1,0:T(8,128)} %get-tuple-element.5) | data formatting | bytes 512 | tf_op jit(solution)/shard_map/layer/pallas_call | solution.py:408
  77.0 1.6 %copy.26 = bf16[1,32,2048]{2,1,0:T(8,128)(2,1)} copy(bf16[1,32,2048]{2,1,0:T(8,128)(2,1)} %bitcast.13) | data formatting | bytes 262144
Async XLA Ops:
  0.6 0.7 copy-start.1
  2.0 1.7 %copy-start = (f32[8,64,16]{1,2,0:T(8,128)S(1)}, f32[8,64,16]{1,2,0:T(8,128)}, u32[]{:S(2)}) copy-start(f32[8,64,16]{1,2,0:T(8,128)} %param.32) | copy-start | bytes 98308
